TPU v7x, 32 devices: a whole 2x2x4 slice. The times are simulated.
32 devices in a mesh: sp: 4 (over y, x), tp: 8 (over z, core).
Axes of the slice: x: 2, y: 2, z: 4, core: 2. Of those that a mesh axis runs over, the one named last changes fastest.
Arguments:
- target: bfloat16 [512, 2048], P('sp'), may hold values from -6 to 6
- source: bfloat16 [1536, 2048], P('sp'), may hold values from -6 to 6
- cotangent: bfloat16 [512, 2048], P('sp'), may hold values from -192 to 192
- target_gain: float32 [2048], replicated, may hold values from 0.1 to 1.9
- source_gain: float32 [2048], replicated, may hold values from 0.1 to 1.9
- w_query: bfloat16 [2048, 4096], P(None, 'tp'), may hold values from -0.125 to 0.125
- w_key: bfloat16 [2048, 128], replicated, may hold values from -0.125 to 0.125
- w_value: bfloat16 [2048, 128], replicated, may hold values from -0.125 to 0.125
- w_out: bfloat16 [4096, 2048], P('tp'), may hold values from -0.09375 to 0.09375
Outputs:
- grad_target: bfloat16 [512, 2048], P(('sp', 'tp'))
- grad_source: bfloat16 [1536, 2048], P(('sp', 'tp'))
- grad_out_w: bfloat16 [4096, 2048], P('tp', 'sp')
All inputs are finite; a program needn't handle non-finite values.
Results may differ from a plain program's by a relative error of at most 0.025.
Values may be sent and summed in bfloat16 or wider, within the bound.
A program may use at most 64 MiB of HBM per device.

v0:
```python
import jax
import jax.numpy as jnp
from jax import lax
from jax.sharding import PartitionSpec as P

HEAD = 128
NORM_EPS = 1e-06
KEY_BLOCK = 1024
QUERY_BLOCK = 256


def normed(row_block, gain_vec):
    rows_wide = row_block.astype(jnp.float32)
    inv_rms = lax.rsqrt(jnp.mean(rows_wide * rows_wide, axis=1, keepdims=True) + NORM_EPS)
    return (rows_wide * inv_rms * gain_vec).astype(jnp.bfloat16)


def norm_back(row_block, gain_vec, upstream):
    rows_wide = row_block.astype(jnp.float32)
    inv_rms = lax.rsqrt(jnp.mean(rows_wide * rows_wide, axis=1, keepdims=True) + NORM_EPS)
    unit_rows = rows_wide * inv_rms
    pulled = upstream * gain_vec
    return inv_rms * (pulled - unit_rows * jnp.mean(pulled * unit_rows, axis=1, keepdims=True))


def block_span(row_count, largest):
    if row_count > largest and row_count % largest == 0:
        return largest
    return row_count


def right_product(left_rows, weight_mat):
    return lax.dot_general(
        left_rows, weight_mat, (((1,), (1,)), ((), ())), preferred_element_type=jnp.float32
    )


def on_device(target, source, cotangent, target_gain, source_gain, w_query, w_key, w_value, w_out):
    tp_count = lax.axis_size("tp")
    tp_place = lax.axis_index("tp")
    group_rows = target.shape[0]
    q_width = w_query.shape[1]
    heads_here = q_width // HEAD
    inv_root = HEAD ** (-0.5)
    query_all = jnp.dot(
        normed(target, target_gain), w_query, preferred_element_type=jnp.float32
    ).astype(jnp.bfloat16)
    grad_all = right_product(cotangent, w_out).astype(jnp.bfloat16)
    cot_columns = lax.all_to_all(cotangent, "sp", split_axis=1, concat_axis=0, tiled=True)
    source_rows = source.shape[0] // tp_count
    source_part = lax.dynamic_slice_in_dim(source, tp_place * source_rows, source_rows, 0)
    source_normed = normed(source_part, source_gain)
    key_own = jnp.dot(source_normed, w_key, preferred_element_type=jnp.float32).astype(jnp.bfloat16)
    value_own = jnp.dot(source_normed, w_value, preferred_element_type=jnp.float32).astype(
        jnp.bfloat16
    )
    key_group, value_group = (
        lax.all_gather(key_own, "tp", axis=0, tiled=True),
        lax.all_gather(value_own, "tp", axis=0, tiled=True),
    )
    query_heads = query_all.reshape(group_rows, heads_here, HEAD)
    grad_heads = grad_all.reshape(group_rows, heads_here, HEAD)
    empty_stat = jnp.zeros((group_rows, heads_here), jnp.float32)
    empty_acc = jnp.zeros((group_rows, heads_here, HEAD), jnp.float32)
    start_state = (empty_stat, empty_acc, empty_acc, empty_acc)
    key_piece = lax.all_gather(key_group, "sp", axis=0, tiled=True)
    value_piece = lax.all_gather(value_group, "sp", axis=0, tiled=True)
    piece_rows = key_piece.shape[0]
    step_rows = block_span(piece_rows, KEY_BLOCK)

    def attend_one_block(block_index, loop_state):
        row_total, output_sum, tilted_sum, weight_sum = loop_state
        key_block = lax.dynamic_slice_in_dim(key_piece, block_index * step_rows, step_rows, 0)
        value_block = lax.dynamic_slice_in_dim(value_piece, block_index * step_rows, step_rows, 0)
        scores = (
            jnp.einsum("ihd,jd->ihj", query_heads, key_block, preferred_element_type=jnp.float32)
            * inv_root
        )
        exponent = jnp.exp(scores)
        weights = exponent.astype(jnp.bfloat16)
        prob_grad = jnp.einsum(
            "ihd,jd->ihj", grad_heads, value_block, preferred_element_type=jnp.float32
        )
        tilted = (exponent * prob_grad).astype(jnp.bfloat16)
        row_total = row_total + jnp.sum(exponent, axis=2)
        output_sum = output_sum + jnp.einsum(
            "ihj,jd->ihd", weights, value_block, preferred_element_type=jnp.float32
        )
        tilted_sum = tilted_sum + jnp.einsum(
            "ihj,jd->ihd", tilted, key_block, preferred_element_type=jnp.float32
        )
        weight_sum = weight_sum + jnp.einsum(
            "ihj,jd->ihd", weights, key_block, preferred_element_type=jnp.float32
        )
        return (row_total, output_sum, tilted_sum, weight_sum)

    row_total, output_sum, tilted_sum, weight_sum = lax.fori_loop(
        0, piece_rows // step_rows, attend_one_block, start_state
    )
    attended = (output_sum / row_total[:, :, None]).astype(jnp.bfloat16)
    delta_row = jnp.sum(attended.astype(jnp.float32) * grad_heads.astype(jnp.float32), axis=2)
    grad_query = (
        (tilted_sum - delta_row[:, :, None] * weight_sum) / row_total[:, :, None] * inv_root
    ).astype(jnp.bfloat16)
    all_total, all_delta = (
        lax.all_gather(row_total, "sp", axis=0, tiled=True),
        lax.all_gather(delta_row, "sp", axis=0, tiled=True),
    )
    empty_keys = jnp.zeros((key_group.shape[0], HEAD), jnp.float32)
    query_piece = lax.all_gather(query_all, "sp", axis=0, tiled=True)
    grad_piece = lax.all_gather(grad_all, "sp", axis=0, tiled=True)
    piece_rows = query_piece.shape[0]
    collect_step_rows = block_span(piece_rows, QUERY_BLOCK)

    def collect_one_block(block_index, loop_state):
        key_grad, value_grad = loop_state
        local_begin = block_index * collect_step_rows
        query_block = lax.dynamic_slice_in_dim(
            query_piece, local_begin, collect_step_rows, 0
        ).reshape(collect_step_rows, heads_here, HEAD)
        grad_block = lax.dynamic_slice_in_dim(
            grad_piece, local_begin, collect_step_rows, 0
        ).reshape(collect_step_rows, heads_here, HEAD)
        total_block = lax.dynamic_slice_in_dim(all_total, local_begin, collect_step_rows, 0)
        delta_block = lax.dynamic_slice_in_dim(all_delta, local_begin, collect_step_rows, 0)
        scores = (
            jnp.einsum("ihd,jd->ihj", query_block, key_group, preferred_element_type=jnp.float32)
            * inv_root
        )
        prob_rows = jnp.exp(scores) / total_block[:, :, None]
        prob_grad = jnp.einsum(
            "ihd,jd->ihj", grad_block, value_group, preferred_element_type=jnp.float32
        )
        score_grad = (prob_rows * (prob_grad - delta_block[:, :, None])).astype(jnp.bfloat16)
        key_grad = (
            key_grad
            + jnp.einsum("ihj,ihd->jd", score_grad, query_block, preferred_element_type=jnp.float32)
            * inv_root
        )
        value_grad = value_grad + jnp.einsum(
            "ihj,ihd->jd",
            prob_rows.astype(jnp.bfloat16),
            grad_block,
            preferred_element_type=jnp.float32,
        )
        return (key_grad, value_grad)

    key_grad, value_grad = lax.fori_loop(
        0, piece_rows // collect_step_rows, collect_one_block, (empty_keys, empty_keys)
    )
    key_sum, value_sum = (
        lax.psum_scatter(
            key_grad.astype(jnp.bfloat16), "tp", scatter_dimension=0, tiled=True
        ).astype(jnp.float32),
        lax.psum_scatter(
            value_grad.astype(jnp.bfloat16), "tp", scatter_dimension=0, tiled=True
        ).astype(jnp.float32),
    )
    pulled_source = right_product(key_sum.astype(jnp.bfloat16), w_key) + right_product(
        value_sum.astype(jnp.bfloat16), w_value
    )
    grad_source = norm_back(source_part, source_gain, pulled_source).astype(jnp.bfloat16)
    query_grad_rows = grad_query.reshape(group_rows, q_width)
    target_rows = group_rows // tp_count
    pulled_target = lax.psum_scatter(
        right_product(query_grad_rows, w_query).astype(jnp.bfloat16),
        "tp",
        scatter_dimension=0,
        tiled=True,
    ).astype(jnp.float32)
    target_part = lax.dynamic_slice_in_dim(target, tp_place * target_rows, target_rows, 0)
    grad_target = norm_back(target_part, target_gain, pulled_target).astype(jnp.bfloat16)
    attended_rows = attended.reshape(group_rows, q_width)
    grad_out = lax.dot_general(
        lax.all_gather(attended_rows, "sp", axis=0, tiled=True),
        cot_columns,
        (((0,), (0,)), ((), ())),
        preferred_element_type=jnp.float32,
    )
    return (grad_target, grad_source, grad_out.astype(jnp.bfloat16))


def solution(mesh):
    in_specs = (
        P("sp", None),
        P("sp", None),
        P("sp", None),
        P(),
        P(),
        P(None, "tp"),
        P(),
        P(),
        P("tp", None),
    )
    out_specs = (P(("sp", "tp"), None), P(("sp", "tp"), None), P("tp", "sp"))
    return jax.shard_map(
        on_device, mesh=mesh, in_specs=in_specs, out_specs=out_specs, check_vma=False
    )
```

profile of v0, /device:TPU:0, one launch (start us, length us, event | category | flops | bytes accessed | tf_op | source)
XLA Modules:
  0.0 221.8 jit_solution(9454115933237955824)
XLA Ops:
  7.3 2.7 %convolution_convert_fusion.2 = bf16[128,512]{1,0:T(8,128)(2,1)S(1)} fusion(bf16[128,2048]{1,0:T(8,128)(2,1)} %param.13, bf16[512,2048]{1,0:T(8,128)(2,1)} %param.19), kind=kOutput, calls=%fused_computation.33 | convolution fusion | flops 268500992 | bytes 2752512 | tf_op jit(solution)/shard_map/dot_general | solution.py:33
  10.1 12.3 %all_gather.33 = bf16[512,512]{1,0:T(8,128)(2,1)} all-gather(bf16[128,512]{1,0:T(8,128)(2,1)S(1)} %convolution_convert_fusion.2), channel_id=1, replica_groups=mesh['sp'=4,'tp'=8] {'sp'}, dimensions={0}, use_global_device_ids=true | all-gather | bytes 655360 | tf_op jit(solution)/shard_map/all_gather | solution.py:111
  24.8 14.1 %all_gather.27 = bf16[384,128]{1,0:T(8,128)(2,1)S(1)} all-gather(bf16[48,128]{1,0:T(8,128)(2,1)S(1)} %convolution_convert_fusion.5), channel_id=1, replica_groups=mesh['sp'=4,'tp'=8] {'tp'}, dimensions={0}, use_global_device_ids=true | all-gather | bytes 110592 | tf_op jit(solution)/shard_map/all_gather | solution.py:58
  38.9 9.4 %all_gather.28 = bf16[1536,128]{1,0:T(8,128)(2,1)S(1)} all-gather(bf16[384,128]{1,0:T(8,128)(2,1)S(1)} %all_gather.27), channel_id=1, replica_groups=mesh['sp'=4,'tp'=8] {'sp'}, dimensions={0}, use_global_device_ids=true | all-gather | bytes 491520 | tf_op jit(solution)/shard_map/all_gather | solution.py:66
  49.0 10.1 %all_gather.31 = bf16[512,512]{1,0:T(8,128)(2,1)} all-gather(bf16[128,512]{1,0:T(8,128)(2,1)S(1)} %convolution_convert_fusion.3), channel_id=1, replica_groups=mesh['sp'=4,'tp'=8] {'sp'}, dimensions={0}, use_global_device_ids=true | all-gather | bytes 655360 | tf_op jit(solution)/shard_map/all_gather | solution.py:110
  60.2 1.4 convolution_convert_fusion.4
  61.6 13.9 %all_gather.29 = bf16[384,128]{1,0:T(8,128)(2,1)S(1)} all-gather(bf16[48,128]{1,0:T(8,128)(2,1)S(1)} %convolution_convert_fusion.4), channel_id=1, replica_groups=mesh['sp'=4,'tp'=8] {'tp'}, dimensions={0}, use_global_device_ids=true | all-gather | bytes 110592 | tf_op jit(solution)/shard_map/all_gather | solution.py:59
  75.5 9.8 %all_gather.30 = bf16[1536,128]{1,0:T(8,128)(2,1)S(1)} all-gather(bf16[384,128]{1,0:T(8,128)(2,1)S(1)} %all_gather.29), channel_id=1, replica_groups=mesh['sp'=4,'tp'=8] {'sp'}, dimensions={0}, use_global_device_ids=true | all-gather | bytes 491520 | tf_op jit(solution)/shard_map/all_gather | solution.py:67
  85.3 6.8 %all_gather.32 = f32[512,4]{0,1:T(4,128)S(1)} all-gather(f32[128,4]{0,1:T(4,128)S(1)} %get-tuple-element.260), channel_id=1, replica_groups=mesh['sp'=4,'tp'=8] {'sp'}, dimensions={0}, use_global_device_ids=true | all-gather | bytes 10240 | tf_op jit(solution)/shard_map/all_gather | solution.py:106
  92.1 1.3 multiply_reduce_fusion
  93.4 8.4 %all_gather.34 = f32[512,4]{0,1:T(4,128)S(1)} all-gather(f32[128,4]{0,1:T(4,128)S(1)} %get-tuple-element.262), channel_id=1, replica_groups=mesh['sp'=4,'tp'=8] {'sp'}, dimensions={0}, use_global_device_ids=true | all-gather | bytes 10240 | tf_op jit(solution)/shard_map/all_gather | solution.py:107
  101.8 16.5 %while.10 = (s32[]{:T(128)}, f32[384,128]{1,0:T(8,128)S(1)}, f32[384,128]{1,0:T(8,128)S(1)}, bf16[512,512]{1,0:T(8,128)(2,1)}, bf16[384,128]{1,0:T(8,128)(2,1)},...) while((s32[]{:T(128)}, f32[384,128]{1,0:T(8,128)S(1)}, ...), condition=%wide.region_8.0_spmd.clone, body=%wide.region_7.0_spmd.clone.sunk | while | flops 405258240 | bytes 8872134 | solution.py:148
  103.0 2.5 %exponential_divide_fusion.2 = f32[256,4,384]{2,0,1:T(8,128)} fusion(bf16[256,4,128]{0,2,1:T(8,128)(2,1)S(1)} %bitcast.95, f32[256,4]{0,1:T(4,128)S(1)} %get-tuple-element.326, bf16[384,128]{1,0:T(8,128)(2,1)} %get-tuple-element.359), kind=kOutput, calls=%fused_computation.1.clone.1 | convolution fusion | flops 101449728 | bytes 1937408 | tf_op jit(solution)/shard_map/while/body/eval_jaxpr/ihd,jd->ihj/dot_general | solution.py:127
  105.7 2.5 %fusion.92 = f32[384,128]{1,0:T(8,128)S(1)} fusion(bf16[256,4,128]{0,2,1:T(8,128)(2,1)S(1)} %bitcast.96, f32[256,4,384]{2,0,1:T(8,128)} %exponential_divide_fusion.2, bf16[256,4,128]{0,2,1:T(8,128)(2,1)S(1)} %bitcast.93, f32[256,4]{0,1:T(4,128)S(1)} %get-tuple-element.328, f32[384,128]{1,0:T(8,128)S(1)} %get-tuple-element.343, ...), kind=kOutput, calls=%fused_computation.6.clone.1 | convolution fusion | flops 202653696 | bytes 2592769 | tf_op jit(solution)/shard_map/while/body/eval_jaxpr/ihj,ihd->jd/dot_general | solution.py:137
  108.2 1.8 fusion.93
  111.3 2.6 %exponential_divide_fusion.2 = f32[256,4,384]{2,0,1:T(8,128)} fusion(bf16[256,4,128]{0,2,1:T(8,128)(2,1)S(1)} %bitcast.95, f32[256,4]{0,1:T(4,128)S(1)} %get-tuple-element.326, bf16[384,128]{1,0:T(8,128)(2,1)} %get-tuple-element.359), kind=kOutput, calls=%fused_computation.1.clone.1 | convolution fusion | flops 101449728 | bytes 1937408 | tf_op jit(solution)/shard_map/while/body/eval_jaxpr/ihd,jd->ihj/dot_general | solution.py:127
  114.0 2.5 %fusion.92 = f32[384,128]{1,0:T(8,128)S(1)} fusion(bf16[256,4,128]{0,2,1:T(8,128)(2,1)S(1)} %bitcast.96, f32[256,4,384]{2,0,1:T(8,128)} %exponential_divide_fusion.2, bf16[256,4,128]{0,2,1:T(8,128)(2,1)S(1)} %bitcast.93, f32[256,4]{0,1:T(4,128)S(1)} %get-tuple-element.328, f32[384,128]{1,0:T(8,128)S(1)} %get-tuple-element.343, ...), kind=kOutput, calls=%fused_computation.6.clone.1 | convolution fusion | flops 202653696 | bytes 2592769 | tf_op jit(solution)/shard_map/while/body/eval_jaxpr/ihj,ihd->jd/dot_general | solution.py:137
  116.5 1.8 fusion.93
  119.0 2.0 copy.45
  121.1 4.1 %all-to-all-start = ((bf16[128,4,512]{0,2,1:T(8,128)(2,1)}), bf16[128,4,512]{0,2,1:T(8,128)(2,1)}, u32[]{:S(2)}, u32[]{:S(2)}) async-start(bf16[128,4,512]{0,2,1:T(8,128)(2,1)} %bitcast.7), calls=%async_computation.3 | async-start | bytes 1048576 | tf_op jit(solution)/shard_map/all_to_all | solution.py:49
  126.0 2.6 %convolution_multiply_fusion.2 = f32[128,4,128]{0,2,1:T(8,128)S(1)} fusion(f32[128,4,1536]{2,0,1:T(8,128)} %copy-done.1, bf16[1536,128]{1,0:T(8,128)(2,1)S(1)} %copy-done.3, f32[128,4]{0,1:T(4,128)S(1)} %get-tuple-element.262), kind=kOutput, calls=%fused_computation.28 | convolution fusion | flops 202178560 | bytes 3803136 | tf_op jit(solution)/shard_map/while/body/eval_jaxpr/ihj,jd->ihd/dot_general | solution.py:92
  128.6 3.6 %fusion.17 = bf16[128,4,128]{0,2,1:T(8,128)(2,1)} fusion(f32[128,4,128]{0,2,1:T(8,128)S(1)} %convolution_multiply_fusion.2, f32[128,4,1536]{2,0,1:T(8,128)} %copy-done.1, bf16[128,4,128]{0,2,1:T(8,128)(2,1)S(1)} %bitcast.98, bf16[1536,128]{1,0:T(8,128)(2,1)S(1)} %copy-done.5, bf16[1536,128]{1,0:T(8,128)(2,1)S(1)} %copy-done.3, ...), kind=kOutput, calls=%fused_computation.32 | convolution fusion | flops 404488192 | bytes 4458496 | tf_op jit(solution)/shard_map/while/body/eval_jaxpr/ihj,jd->ihd/dot_general | solution.py:89
  132.2 2.6 %convolution_convert_fusion = bf16[128,2048]{1,0:T(8,128)(2,1)} fusion(bf16[128,512]{0,1:T(8,128)(2,1)} %bitcast.100, bf16[2048,512]{1,0:T(8,128)(2,1)S(1)} %copy-done), kind=kOutput, calls=%fused_computation.20 | convolution fusion | flops 268697600 | bytes 2752512 | tf_op jit(solution)/shard_map/dot_general | solution.py:33
  136.4 10.5 %all_gather.35 = bf16[512,512]{0,1:T(8,128)(2,1)S(1)} all-gather(bf16[128,512]{0,1:T(8,128)(2,1)S(1)} %bitcast.99), channel_id=1, replica_groups=mesh['sp'=4,'tp'=8] {'sp'}, dimensions={0}, use_global_device_ids=true | all-gather | bytes 655360 | tf_op jit(solution)/shard_map/all_gather | solution.py:175
  146.9 2.9 %reduce-scatter.6.cloned.1.call-done = bf16[48,128]{1,0:T(8,128)(2,1)} async-done(((bf16[384,128]{1,0:T(8,128)(2,1)}), bf16[48,128]{1,0:T(8,128)(2,1)}) %reduce-scatter.6.cloned.1.call-update) | async-done | bytes 12304 | tf_op jit(solution)/shard_map/reduce_scatter | solution.py:152
  149.8 1.3 fusion.56
  151.1 29.6 %reduce-scatter.8.cloned.1.call-done = bf16[48,128]{1,0:T(8,128)(2,1)} async-done(((bf16[384,128]{1,0:T(8,128)(2,1)}), bf16[48,128]{1,0:T(8,128)(2,1)}) %reduce-scatter.8.cloned.1.call-update) | async-done | bytes 12304 | tf_op jit(solution)/shard_map/reduce_scatter | solution.py:155
  180.7 1.3 fusion.31
  182.1 1.8 fusion.34
  183.9 1.2 copy.46
  186.4 26.2 %reduce-scatter.4.cloned.1.call-done = bf16[16,2048]{1,0:T(8,128)(2,1)} async-done(((bf16[128,2048]{1,0:T(8,128)(2,1)}), bf16[16,2048]{1,0:T(8,128)(2,1)}) %reduce-scatter.4.cloned.1.call-update) | async-done | bytes 65552 | tf_op jit(solution)/shard_map/reduce_scatter | solution.py:165
  213.7 1.6 fusion.47
  (65 shorter events, 12.3 us)
Async XLA Ops:
  7.2 41.4 %copy-start = (bf16[2048,512]{1,0:T(8,128)(2,1)S(1)}, bf16[2048,512]{1,0:T(8,128)(2,1)}, u32[]{:S(2)}) copy-start(bf16[2048,512]{1,0:T(8,128)(2,1)} %param.16) | copy-start | bytes 6291460
  7.2 142.6 %reduce-scatter.6.cloned.1.call-start = ((), (), s32[]{:S(2)}) async-start(), calls=%async_computation.5 | async-start | bytes 110592 | tf_op jit(solution)/shard_map/reduce_scatter | solution.py:152
  7.2 16.3 %copy-start.8 = (bf16[2048,128]{1,0:T(8,128)(2,1)S(1)}, bf16[2048,128]{1,0:T(8,128)(2,1)}, u32[]{:S(2)}) copy-start(bf16[2048,128]{1,0:T(8,128)(2,1)} %param.17) | copy-start | bytes 1572868
  7.3 16.3 %copy-start.12 = (f32[2048]{0:T(1024)S(1)}, f32[2048]{0:T(1024)}, u32[]{:S(2)}) copy-start(f32[2048]{0:T(1024)} %param.15) | copy-start | bytes 24580
  10.0 38.5 %copy-start.13 = (f32[2048]{0:T(1024)S(1)}, f32[2048]{0:T(1024)}, u32[]{:S(2)}) copy-start(f32[2048]{0:T(1024)} %param.14) | copy-start | bytes 24580
  22.4 25.9 %copy-start.9 = (bf16[128,2048]{1,0:T(8,128)(2,1)S(1)}, bf16[128,2048]{1,0:T(8,128)(2,1)}, u32[]{:S(2)}) copy-start(bf16[128,2048]{1,0:T(8,128)(2,1)} %param.11) | copy-start | bytes 1572868
  23.6 36.3 %copy-start.14 = (f32[48]{0:T(128)}, f32[48]{0:T(128)S(1)}, u32[]{:S(2)}) copy-start(f32[48]{0:T(128)S(1)} %add_rsqrt_fusion) | copy-start | bytes 580
  38.9 9.6 %copy-start.11 = (bf16[384,128]{1,0:T(8,128)(2,1)}, bf16[384,128]{1,0:T(8,128)(2,1)S(1)}, u32[]{:S(2)}) copy-start(bf16[384,128]{1,0:T(8,128)(2,1)S(1)} %all_gather.27) | copy-start | bytes 294916
  48.3 10.8 %copy-start.2 = (bf16[1536,128]{1,0:T(8,128)(2,1)}, bf16[1536,128]{1,0:T(8,128)(2,1)S(1)}, u32[]{:S(2)}) copy-start(bf16[1536,128]{1,0:T(8,128)(2,1)S(1)} %all_gather.28) | copy-start | bytes 1179652
  59.1 1.0 copy-start.6
  60.2 33.3 %copy-start.1 = (f32[128,4,1536]{2,0,1:T(8,128)}, f32[128,4,1536]{2,0,1:T(8,128)S(1)}, u32[]{:S(2)}) copy-start(f32[128,4,1536]{2,0,1:T(8,128)S(1)} %get-tuple-element.261) | copy-start | bytes 9437188
  85.3 8.1 %copy-start.4 = (bf16[1536,128]{1,0:T(8,128)(2,1)}, bf16[1536,128]{1,0:T(8,128)(2,1)S(1)}, u32[]{:S(2)}) copy-start(bf16[1536,128]{1,0:T(8,128)(2,1)S(1)} %all_gather.30) | copy-start | bytes 1179652
  118.3 7.7 %copy-start.3 = (bf16[1536,128]{1,0:T(8,128)(2,1)S(1)}, bf16[1536,128]{1,0:T(8,128)(2,1)}, u32[]{:S(2)}) copy-start(bf16[1536,128]{1,0:T(8,128)(2,1)} %copy-done.2) | copy-start | bytes 1179652
  121.1 62.8 %all-to-all-start = ((bf16[128,4,512]{0,2,1:T(8,128)(2,1)}), bf16[128,4,512]{0,2,1:T(8,128)(2,1)}, u32[]{:S(2)}, u32[]{:S(2)}) async-start(bf16[128,4,512]{0,2,1:T(8,128)(2,1)} %bitcast.7), calls=%async_computation.3 | async-start | bytes 1048576 | tf_op jit(solution)/shard_map/all_to_all | solution.py:49
  125.2 55.6 %reduce-scatter.8.cloned.1.call-start = ((), (), s32[]{:S(2)}) async-start(), calls=%async_computation.6 | async-start | bytes 110592 | tf_op jit(solution)/shard_map/reduce_scatter | solution.py:155
  125.9 2.7 %copy-start.5 = (bf16[1536,128]{1,0:T(8,128)(2,1)S(1)}, bf16[1536,128]{1,0:T(8,128)(2,1)}, u32[]{:S(2)}) copy-start(bf16[1536,128]{1,0:T(8,128)(2,1)} %copy-done.4) | copy-start | bytes 1179652
  126.0 86.7 %reduce-scatter.4.cloned.1.call-start = ((), (), s32[]{:S(2)}) async-start(), calls=%async_computation.4 | async-start | bytes 589824 | tf_op jit(solution)/shard_map/reduce_scatter | solution.py:165
  132.2 4.1 %copy-start.10 = (bf16[128,4,128]{0,2,1:T(8,128)(2,1)S(1)}, bf16[128,4,128]{0,2,1:T(8,128)(2,1)}, u32[]{:S(2)}) copy-start(bf16[128,4,128]{0,2,1:T(8,128)(2,1)} %get-tuple-element.263) | copy-start | bytes 393220
  134.8 46.0 %copy-start.7 = (bf16[2048,128]{1,0:T(8,128)(2,1)S(1)}, bf16[2048,128]{1,0:T(8,128)(2,1)}, u32[]{:S(2)}) copy-start(bf16[2048,128]{1,0:T(8,128)(2,1)} %param.18) | copy-start | bytes 1572868
  182.1 30.5 %copy-start.15 = (f32[16]{0:T(128)S(1)}, f32[16]{0:T(128)}, u32[]{:S(2)}) copy-start(f32[16]{0:T(128)} %add_rsqrt_fusion.2) | copy-start | bytes 196
Sparse Core Ops, SparseCore 0:
  119.1 30.5 reduce-scatter.5
  152.0 28.7 reduce-scatter.7
  183.0 29.5 reduce-scatter.3
where the time goes:
time: 223 us; the launch traced here: 222 us
  blocking collectives  95.2 us (43%)
  waiting for transfers between devices  58.9 us (26%)
  matrix products  34.2 us (15%)
  between operations  14 us (6%)
  other arithmetic  8.6 us (4%)
  local copies, waits for them, and re-layouts  6.51 us (3%)
  starting transfers between devices  4.25 us (2%)
    reduce_scatter x1, waiting for transfers between devices, on_device(): lax.psum_scatter(value_grad.astype(jnp.bfloat16), 'tp', scatter_dimension...  29.6 us
    reduce_scatter x1, waiting for transfers between devices, on_device(): lax.psum_scatter(right_product(query_grad_rows, w_query).astype(jnp.bfloa...  26.2 us
    all_gather x1, blocking collectives, on_device(): lax.all_gather(key_own, 'tp', axis=0, tiled=True)  14.1 us
    all_gather x1, blocking collectives, on_device(): lax.all_gather(value_own, 'tp', axis=0, tiled=True)  13.9 us
    all_gather x1, blocking collectives, on_device(): grad_piece = lax.all_gather(grad_all, 'sp', axis=0, tiled=True)  12.3 us
    all_gather x1, blocking collectives, on_device(): lax.all_gather(attended_rows, 'sp', axis=0, tiled=True)  10.5 us
    all_gather x1, blocking collectives, on_device(): query_piece = lax.all_gather(query_all, 'sp', axis=0, tiled=True)  10.1 us
    all_gather x1, blocking collectives, on_device(): value_piece = lax.all_gather(value_group, 'sp', axis=0, tiled=True)  9.79 us
  transfers between devices with their start and end apart: 4, of which 3 were waited for; matrix products, arithmetic and copies ran while one was open for 9% of the time, Pallas kernels for 0%

commit v1 on v0

--- a/solution.py
+++ b/solution.py
@@ -108,7 +108,13 @@
     )
     empty_keys = jnp.zeros((key_group.shape[0], HEAD), jnp.float32)
     query_piece = lax.all_gather(query_all, "sp", axis=0, tiled=True)
-    grad_piece = lax.all_gather(grad_all, "sp", axis=0, tiled=True)
+    size = lax.axis_size("sp")
+    held, parts = (grad_all, [grad_all])
+    for _ in range(size - 1):
+        held = lax.ppermute(held, "sp", [(i, (i + 1) % size) for i in range(size)])
+        parts.insert(0, held)
+    line = jnp.concatenate(parts, axis=0)
+    grad_piece = jnp.roll(line, (lax.axis_index("sp") + 1) * grad_all.shape[0], axis=0)
     piece_rows = query_piece.shape[0]
     collect_step_rows = block_span(piece_rows, QUERY_BLOCK)
 

time: 223 us -> 230 us (1.031)
  blocking collectives: 95.2 us -> 83.8 us
  waiting for transfers between devices: 58.9 us -> 70.2 us
  starting transfers between devices: 4.25 us -> 8.03 us
    all_gather x1 -> x0, blocking collectives: 12.3 us -> none  [on_device(): grad_piece = lax.all_gather(grad_all, 'sp', axis=0, tiled=True)]
    reduce_scatter x1, waiting for transfers between devices: 2.91 us -> 9.84 us  [on_device(): lax.psum_scatter(key_grad.astype(jnp.bfloat16), 'tp', scatter_dimension=0...]
    ppermute x0 -> x3, starting transfers between devices: none -> 3.64 us  [on_device(): held = lax.ppermute(held, 'sp', [(i, (i + 1) % size) for i in range(size)])]
  transfers between devices with their start and end apart: 4 -> 7, of which waited for: 3 -> 4; matrix products, arithmetic and copies ran while one was open for 9% -> 21% of each run, Pallas kernels for 0% -> 0%
where the time goes in v1:
time: 230 us; the launch traced here: 229 us
  blocking collectives  83.8 us (36%)
  waiting for transfers between devices  70.2 us (31%)
  matrix products  36.1 us (16%)
  between operations  14.1 us (6%)
  local copies, waits for them, and re-layouts  8.73 us (4%)
  starting transfers between devices  8.03 us (3%)
  other arithmetic  7.97 us (3%)
    reduce_scatter x1, waiting for transfers between devices, on_device(): lax.psum_scatter(value_grad.astype(jnp.bfloat16), 'tp', scatter_dimension...  29.7 us
    reduce_scatter x1, waiting for transfers between devices, on_device(): lax.psum_scatter(right_product(query_grad_rows, w_query).astype(jnp.bfloa...  28.5 us
    all_gather x1, blocking collectives, on_device(): lax.all_gather(key_own, 'tp', axis=0, tiled=True)  14.2 us
    all_gather x1, blocking collectives, on_device(): lax.all_gather(value_own, 'tp', axis=0, tiled=True)  13.9 us
    all_gather x1, blocking collectives, on_device(): lax.all_gather(attended_rows, 'sp', axis=0, tiled=True)  9.93 us
    all_gather x1, blocking collectives, on_device(): key_piece = lax.all_gather(key_group, 'sp', axis=0, tiled=True)  9.91 us
    reduce_scatter x1, waiting for transfers between devices, on_device(): lax.psum_scatter(key_grad.astype(jnp.bfloat16), 'tp', scatter_dimension=0...  9.84 us
    all_gather x1, blocking collectives, on_device(): query_piece = lax.all_gather(query_all, 'sp', axis=0, tiled=True)  9.79 us
  transfers between devices with their start and end apart: 7, of which 4 were waited for; matrix products, arithmetic and copies ran while one was open for 21% of the time, Pallas kernels for 0%

profile of v1, /device:TPU:0, one launch (start us, length us, event | category | flops | bytes accessed | tf_op | source)
XLA Modules:
  0.0 229.0 jit_solution(1760139788541956099)
XLA Ops:
  7.2 2.7 %convolution_convert_fusion.2 = bf16[128,512]{1,0:T(8,128)(2,1)S(1)} fusion(bf16[128,2048]{1,0:T(8,128)(2,1)} %param.13, bf16[512,2048]{1,0:T(8,128)(2,1)} %param.19), kind=kOutput, calls=%fused_computation.33 | convolution fusion | flops 268500992 | bytes 2752512 | tf_op jit(solution)/shard_map/dot_general | solution.py:33
  10.0 3.0 %collective-permute-start = (bf16[128,512]{1,0:T(8,128)(2,1)S(1)}, bf16[128,512]{1,0:T(8,128)(2,1)}, u32[]{:S(2)}, u32[]{:S(2)}) collective-permute-start(bf16[128,512]{1,0:T(8,128)(2,1)S(1)} %convolution_convert_fusion.2), channel_id=1, source_target_pairs={{0,8},{8,16},{16,24},{24,0},{1,9},{9,17},{17,25},{25,1},{2,10},{10... | collective-permute-start | bytes 393224 | tf_op jit(solution)/shard_map/ppermute | solution.py:114
  14.0 4.3 %all-to-all-start = ((bf16[128,4,512]{0,2,1:T(8,128)(2,1)}), bf16[128,4,512]{0,2,1:T(8,128)(2,1)}, u32[]{:S(2)}, u32[]{:S(2)}) async-start(bf16[128,4,512]{0,2,1:T(8,128)(2,1)} %bitcast.7), calls=%async_computation.3 | async-start | bytes 1048576 | tf_op jit(solution)/shard_map/all_to_all | solution.py:49
  20.6 14.2 %all_gather.24 = bf16[384,128]{1,0:T(8,128)(2,1)S(1)} all-gather(bf16[48,128]{1,0:T(8,128)(2,1)S(1)} %convolution_convert_fusion.5), channel_id=1, replica_groups=mesh['sp'=4,'tp'=8] {'tp'}, dimensions={0}, use_global_device_ids=true | all-gather | bytes 110592 | tf_op jit(solution)/shard_map/all_gather | solution.py:58
  34.8 9.9 %all_gather.25 = bf16[1536,128]{1,0:T(8,128)(2,1)S(1)} all-gather(bf16[384,128]{1,0:T(8,128)(2,1)S(1)} %all_gather.24), channel_id=1, replica_groups=mesh['sp'=4,'tp'=8] {'sp'}, dimensions={0}, use_global_device_ids=true | all-gather | bytes 491520 | tf_op jit(solution)/shard_map/all_gather | solution.py:66
  45.5 2.3 fusion.55
  49.1 13.9 %all_gather.26 = bf16[384,128]{1,0:T(8,128)(2,1)S(1)} all-gather(bf16[48,128]{1,0:T(8,128)(2,1)S(1)} %convolution_convert_fusion.4), channel_id=1, replica_groups=mesh['sp'=4,'tp'=8] {'tp'}, dimensions={0}, use_global_device_ids=true | all-gather | bytes 110592 | tf_op jit(solution)/shard_map/all_gather | solution.py:59
  63.0 9.4 %all_gather.27 = bf16[1536,128]{1,0:T(8,128)(2,1)S(1)} all-gather(bf16[384,128]{1,0:T(8,128)(2,1)S(1)} %all_gather.26), channel_id=1, replica_groups=mesh['sp'=4,'tp'=8] {'sp'}, dimensions={0}, use_global_device_ids=true | all-gather | bytes 491520 | tf_op jit(solution)/shard_map/all_gather | solution.py:67
  73.1 3.4 %multiply_reduce_fusion = (f32[128,4]{0,1:T(4,128)S(1)}, bf16[128,4,128]{0,2,1:T(8,128)(2,1)}) fusion(bf16[128,512]{0,1:T(8,128)(2,1)S(1)} %copy.61, f32[128,4]{0,1:T(4,128)S(1)} %get-tuple-element.260, bf16[1536,128]{1,0:T(8,128)(2,1)S(1)} %all_gather.27, f32[128,4,1536]{2,0,1:T(8,128)} %get-tuple-element.261), kind=kOutput, calls=%fused_computation.61 | convolution fusion | flops 202505728 | bytes 3805184 | tf_op jit(solution)/shard_map/while/body/eval_jaxpr/ihj,jd->ihd/dot_general | solution.py:86
  76.4 2.1 collective-permute-done.1
  78.6 1.4 convolution_multiply_fusion.2
  80.0 8.6 %all_gather.29 = f32[512,4]{0,1:T(4,128)S(1)} all-gather(f32[128,4]{0,1:T(4,128)S(1)} %get-tuple-element.260), channel_id=1, replica_groups=mesh['sp'=4,'tp'=8] {'sp'}, dimensions={0}, use_global_device_ids=true | all-gather | bytes 10240 | tf_op jit(solution)/shard_map/all_gather | solution.py:106
  88.6 8.1 %all_gather.30 = f32[512,4]{0,1:T(4,128)S(1)} all-gather(f32[128,4]{0,1:T(4,128)S(1)} %get-tuple-element.262), channel_id=1, replica_groups=mesh['sp'=4,'tp'=8] {'sp'}, dimensions={0}, use_global_device_ids=true | all-gather | bytes 10240 | tf_op jit(solution)/shard_map/all_gather | solution.py:107
  96.6 9.8 %all_gather.28 = bf16[512,512]{1,0:T(8,128)(2,1)} all-gather(bf16[128,512]{1,0:T(8,128)(2,1)S(1)} %copy-done.11), channel_id=1, replica_groups=mesh['sp'=4,'tp'=8] {'sp'}, dimensions={0}, use_global_device_ids=true | all-gather | bytes 655360 | tf_op jit(solution)/shard_map/all_gather | solution.py:110
  109.2 16.5 %while.10 = (s32[]{:T(128)}, f32[384,128]{1,0:T(8,128)S(1)}, f32[384,128]{1,0:T(8,128)S(1)}, bf16[512,512]{1,0:T(8,128)(2,1)}, bf16[384,128]{1,0:T(8,128)(2,1)},...) while((s32[]{:T(128)}, f32[384,128]{1,0:T(8,128)S(1)}, ...), condition=%wide.region_8.9_spmd.clone, body=%wide.region_7.8_spmd.clone.sunk | while | flops 405258240 | bytes 8872134 | solution.py:154
  110.4 2.6 %exponential_divide_fusion.2 = f32[256,4,384]{2,0,1:T(8,128)} fusion(bf16[256,4,128]{0,2,1:T(8,128)(2,1)S(1)} %bitcast.95, f32[256,4]{0,1:T(4,128)S(1)} %get-tuple-element.326, bf16[384,128]{1,0:T(8,128)(2,1)} %get-tuple-element.359), kind=kOutput, calls=%fused_computation.1.clone.1 | convolution fusion | flops 101449728 | bytes 1937408 | tf_op jit(solution)/shard_map/while/body/eval_jaxpr/ihd,jd->ihj/dot_general | solution.py:133
  113.1 2.5 %fusion.92 = f32[384,128]{1,0:T(8,128)S(1)} fusion(bf16[256,4,128]{0,2,1:T(8,128)(2,1)S(1)} %bitcast.96, f32[256,4,384]{2,0,1:T(8,128)} %exponential_divide_fusion.2, bf16[256,4,128]{0,2,1:T(8,128)(2,1)S(1)} %bitcast.93, f32[256,4]{0,1:T(4,128)S(1)} %get-tuple-element.328, f32[384,128]{1,0:T(8,128)S(1)} %get-tuple-element.343, ...), kind=kOutput, calls=%fused_computation.6.clone.1 | convolution fusion | flops 202653696 | bytes 2592769 | tf_op jit(solution)/shard_map/while/body/eval_jaxpr/ihj,ihd->jd/dot_general | solution.py:143
  115.6 1.8 fusion.93
  118.7 2.6 %exponential_divide_fusion.2 = f32[256,4,384]{2,0,1:T(8,128)} fusion(bf16[256,4,128]{0,2,1:T(8,128)(2,1)S(1)} %bitcast.95, f32[256,4]{0,1:T(4,128)S(1)} %get-tuple-element.326, bf16[384,128]{1,0:T(8,128)(2,1)} %get-tuple-element.359), kind=kOutput, calls=%fused_computation.1.clone.1 | convolution fusion | flops 101449728 | bytes 1937408 | tf_op jit(solution)/shard_map/while/body/eval_jaxpr/ihd,jd->ihj/dot_general | solution.py:133
  121.4 2.5 %fusion.92 = f32[384,128]{1,0:T(8,128)S(1)} fusion(bf16[256,4,128]{0,2,1:T(8,128)(2,1)S(1)} %bitcast.96, f32[256,4,384]{2,0,1:T(8,128)} %exponential_divide_fusion.2, bf16[256,4,128]{0,2,1:T(8,128)(2,1)S(1)} %bitcast.93, f32[256,4]{0,1:T(4,128)S(1)} %get-tuple-element.328, f32[384,128]{1,0:T(8,128)S(1)} %get-tuple-element.343, ...), kind=kOutput, calls=%fused_computation.6.clone.1 | convolution fusion | flops 202653696 | bytes 2592769 | tf_op jit(solution)/shard_map/while/body/eval_jaxpr/ihj,ihd->jd/dot_general | solution.py:143
  123.9 1.8 fusion.93
  126.5 3.2 %fusion.17 = bf16[128,4,128]{0,2,1:T(8,128)(2,1)S(1)} fusion(f32[128,4,128]{0,2,1:T(8,128)} %convolution_multiply_fusion.2, f32[128,4,1536]{2,0,1:T(8,128)} %get-tuple-element.261, bf16[128,4,128]{0,2,1:T(8,128)(2,1)S(1)} %bitcast.98, bf16[1536,128]{1,0:T(8,128)(2,1)} %copy-done.3, bf16[1536,128]{1,0:T(8,128)(2,1)} %copy-done.2, ...), kind=kOutput, calls=%fused_computation.32 | convolution fusion | flops 404488192 | bytes 4458496 | tf_op jit(solution)/shard_map/while/body/eval_jaxpr/ihj,jd->ihd/dot_general | solution.py:89
  130.4 1.6 convolution_convert_fusion
  133.0 9.9 %all_gather.31 = bf16[512,512]{0,1:T(8,128)(2,1)S(1)} all-gather(bf16[128,512]{0,1:T(8,128)(2,1)S(1)} %bitcast.99), channel_id=1, replica_groups=mesh['sp'=4,'tp'=8] {'sp'}, dimensions={0}, use_global_device_ids=true | all-gather | bytes 655360 | tf_op jit(solution)/shard_map/all_gather | solution.py:181
  143.0 2.1 copy.46
  145.1 2.3 convolution_convert_fusion.1
  147.3 9.8 %reduce-scatter.6.cloned.1.call-done = bf16[48,128]{1,0:T(8,128)(2,1)} async-done(((bf16[384,128]{1,0:T(8,128)(2,1)}), bf16[48,128]{1,0:T(8,128)(2,1)}) %reduce-scatter.6.cloned.1.call-update) | async-done | bytes 12304 | tf_op jit(solution)/shard_map/reduce_scatter | solution.py:158
  157.2 1.3 fusion.56
  158.5 29.7 %reduce-scatter.8.cloned.1.call-done = bf16[48,128]{1,0:T(8,128)(2,1)} async-done(((bf16[384,128]{1,0:T(8,128)(2,1)}), bf16[48,128]{1,0:T(8,128)(2,1)}) %reduce-scatter.8.cloned.1.call-update) | async-done | bytes 12304 | tf_op jit(solution)/shard_map/reduce_scatter | solution.py:161
  189.6 1.7 fusion.34
  191.3 28.5 %reduce-scatter.4.cloned.1.call-done = bf16[16,2048]{1,0:T(8,128)(2,1)} async-done(((bf16[128,2048]{1,0:T(8,128)(2,1)}), bf16[16,2048]{1,0:T(8,128)(2,1)}) %reduce-scatter.4.cloned.1.call-update) | async-done | bytes 65552 | tf_op jit(solution)/shard_map/reduce_scatter | solution.py:171
  220.9 1.6 fusion.47
  (77 shorter events, 16.3 us)
Async XLA Ops:
  7.2 37.8 %copy-start = (bf16[2048,512]{1,0:T(8,128)(2,1)S(1)}, bf16[2048,512]{1,0:T(8,128)(2,1)}, u32[]{:S(2)}) copy-start(bf16[2048,512]{1,0:T(8,128)(2,1)} %param.16) | copy-start | bytes 6291460
  7.2 5.8 %copy-start.7 = (bf16[128,2048]{1,0:T(8,128)(2,1)S(1)}, bf16[128,2048]{1,0:T(8,128)(2,1)}, u32[]{:S(2)}) copy-start(bf16[128,2048]{1,0:T(8,128)(2,1)} %param.13) | copy-start | bytes 1572868
  9.9 9.5 %copy-start.6 = (bf16[2048,128]{1,0:T(8,128)(2,1)S(1)}, bf16[2048,128]{1,0:T(8,128)(2,1)}, u32[]{:S(2)}) copy-start(bf16[2048,128]{1,0:T(8,128)(2,1)} %param.17) | copy-start | bytes 1572868
  9.9 9.5 %copy-start.13 = (f32[2048]{0:T(1024)S(1)}, f32[2048]{0:T(1024)}, u32[]{:S(2)}) copy-start(f32[2048]{0:T(1024)} %param.15) | copy-start | bytes 24580
  10.0 62.5 %collective-permute-start = (bf16[128,512]{1,0:T(8,128)(2,1)S(1)}, bf16[128,512]{1,0:T(8,128)(2,1)}, u32[]{:S(2)}, u32[]{:S(2)}) collective-permute-start(bf16[128,512]{1,0:T(8,128)(2,1)S(1)} %convolution_convert_fusion.2), channel_id=1, source_target_pairs={{0,8},{8,16},{16,24},{24,0},{1,9},{9,17},{17,25},{25,1},{2,10},{10... | collective-permute-start | bytes 393224 | tf_op jit(solution)/shard_map/ppermute | solution.py:114
  14.0 30.7 %copy-start.8 = (bf16[128,2048]{1,0:T(8,128)(2,1)S(1)}, bf16[128,2048]{1,0:T(8,128)(2,1)}, u32[]{:S(2)}) copy-start(bf16[128,2048]{1,0:T(8,128)(2,1)} %param.11) | copy-start | bytes 1572868
  14.0 30.9 %copy-start.14 = (f32[2048]{0:T(1024)S(1)}, f32[2048]{0:T(1024)}, u32[]{:S(2)}) copy-start(f32[2048]{0:T(1024)} %param.14) | copy-start | bytes 24580
  14.0 128.9 %all-to-all-start = ((bf16[128,4,512]{0,2,1:T(8,128)(2,1)}), bf16[128,4,512]{0,2,1:T(8,128)(2,1)}, u32[]{:S(2)}, u32[]{:S(2)}) async-start(bf16[128,4,512]{0,2,1:T(8,128)(2,1)} %bitcast.7), calls=%async_computation.3 | async-start | bytes 1048576 | tf_op jit(solution)/shard_map/all_to_all | solution.py:49
  18.3 138.9 %reduce-scatter.6.cloned.1.call-start = ((), (), s32[]{:S(2)}) async-start(), calls=%async_computation.5 | async-start | bytes 110592 | tf_op jit(solution)/shard_map/reduce_scatter | solution.py:158
  34.8 10.1 %copy-start.12 = (bf16[384,128]{1,0:T(8,128)(2,1)}, bf16[384,128]{1,0:T(8,128)(2,1)S(1)}, u32[]{:S(2)}) copy-start(bf16[384,128]{1,0:T(8,128)(2,1)S(1)} %all_gather.24) | copy-start | bytes 294916
  44.7 33.9 %copy-start.2 = (bf16[1536,128]{1,0:T(8,128)(2,1)}, bf16[1536,128]{1,0:T(8,128)(2,1)S(1)}, u32[]{:S(2)}) copy-start(bf16[1536,128]{1,0:T(8,128)(2,1)S(1)} %all_gather.25) | copy-start | bytes 1179652
  45.4 2.3 %copy-start.10 = (bf16[128,512]{1,0:T(8,128)(2,1)}, bf16[128,512]{1,0:T(8,128)(2,1)S(1)}, u32[]{:S(2)}) copy-start(bf16[128,512]{1,0:T(8,128)(2,1)S(1)} %convolution_convert_fusion.3) | copy-start | bytes 393220
  45.5 2.3 copy-start.4
  72.4 4.0 %copy-start.3 = (bf16[1536,128]{1,0:T(8,128)(2,1)}, bf16[1536,128]{1,0:T(8,128)(2,1)S(1)}, u32[]{:S(2)}) copy-start(bf16[1536,128]{1,0:T(8,128)(2,1)S(1)} %all_gather.27) | copy-start | bytes 1179652
  72.5 6.1 %collective-permute-start.1 = (bf16[128,512]{1,0:T(8,128)(2,1)}, bf16[128,512]{1,0:T(8,128)(2,1)S(1)}, u32[]{:S(2)}, u32[]{:S(2)}) collective-permute-start(bf16[128,512]{1,0:T(8,128)(2,1)} %collective-permute-done), channel_id=1, source_target_pairs={{0,8},{8,16},{16,24},{24,0},{1,9},{9,17},{17,25},{25,1},{2,10},{10... | collective-permute-start | bytes 393224 | tf_op jit(solution)/shard_map/ppermute | solution.py:114
  73.1 5.5 %copy-start.1 = (f32[128,4,1536]{2,0,1:T(8,128)S(1)}, f32[128,4,1536]{2,0,1:T(8,128)}, u32[]{:S(2)}) copy-start(f32[128,4,1536]{2,0,1:T(8,128)} %get-tuple-element.261) | copy-start | bytes 9437188
  78.6 27.8 %collective-permute-start.2 = (bf16[128,512]{1,0:T(8,128)(2,1)S(1)}, bf16[128,512]{1,0:T(8,128)(2,1)S(1)}, u32[]{:S(2)}, u32[]{:S(2)}) collective-permute-start(bf16[128,512]{1,0:T(8,128)(2,1)S(1)} %collective-permute-done.1), channel_id=1, source_target_pairs={{0,8},{8,16},{16,24},{24,0},{1,9},{9,17},{17,25},{25,1},{2,10},{10... | collective-permute-start | bytes 393224 | tf_op jit(solution)/shard_map/ppermute | solution.py:114
  78.6 18.0 %copy-start.11 = (bf16[128,512]{1,0:T(8,128)(2,1)S(1)}, bf16[128,512]{1,0:T(8,128)(2,1)}, u32[]{:S(2)}) copy-start(bf16[128,512]{1,0:T(8,128)(2,1)} %copy-done.10) | copy-start | bytes 393220
  126.4 61.8 %reduce-scatter.8.cloned.1.call-start = ((), (), s32[]{:S(2)}) async-start(), calls=%async_computation.6 | async-start | bytes 110592 | tf_op jit(solution)/shard_map/reduce_scatter | solution.py:161
  130.3 89.5 %reduce-scatter.4.cloned.1.call-start = ((), (), s32[]{:S(2)}) async-start(), calls=%async_computation.4 | async-start | bytes 589824 | tf_op jit(solution)/shard_map/reduce_scatter | solution.py:171
  130.4 2.6 %copy-start.9 = (bf16[128,4,128]{0,2,1:T(8,128)(2,1)S(1)}, bf16[128,4,128]{0,2,1:T(8,128)(2,1)}, u32[]{:S(2)}) copy-start(bf16[128,4,128]{0,2,1:T(8,128)(2,1)} %get-tuple-element.263) | copy-start | bytes 393220
  143.0 45.2 %copy-start.5 = (bf16[2048,128]{1,0:T(8,128)(2,1)S(1)}, bf16[2048,128]{1,0:T(8,128)(2,1)}, u32[]{:S(2)}) copy-start(bf16[2048,128]{1,0:T(8,128)(2,1)} %param.18) | copy-start | bytes 1572868
Sparse Core Ops, SparseCore 0:
  126.5 30.6 reduce-scatter.5
  159.4 28.7 reduce-scatter.7
  190.5 29.2 reduce-scatter.3
